TPU v7x, 32 devices: a whole 2x2x4 slice. The times are simulated.
32 devices in a mesh: ep: 8 (over z, x), tp: 4 (over y, core).
Axes of the slice: x: 2, y: 2, z: 4, core: 2. Of those that a mesh axis runs over, the one named last changes fastest.
Arguments:
- tokens: bfloat16 [1024, 4096], P('ep', 'tp'), may hold values from -16 to 16
- expert_ids: int32 [1024, 2], P('ep'), may hold values from 0 to 7, as said below
- group_weight: float32 [1024], P('ep'), may hold values from 0.25 to 1
- expert_weight: float32 [1024, 2], P('ep'), may hold values from 0.1 to 1
- w_gate: bfloat16 [8, 4096, 512], P('ep', None, 'tp'), may hold values from -0.09375 to 0.09375
- w_up: bfloat16 [8, 4096, 512], P('ep', None, 'tp'), may hold values from -0.09375 to 0.09375
- w_down: bfloat16 [8, 512, 4096], P('ep', None, 'tp'), may hold values from -0.5 to 0.5
- norm_gain: float32 [4096], P('tp'), may hold values from 0.1 to 1.9
- norm_bias: float32 [4096], P('tp'), may hold values from -3 to 3
Outputs:
- normed: bfloat16 [1024, 4096], P('ep', 'tp')
Inputs may be any that keep to these rules, and one draw needn't show every extreme that they name: `expert_ids`: each row names 2 different experts of one group, a group being 2 consecutive ids; in the rows of one ep index each group is named by a 4-th of the rows. In the rows of one ep index no expert is named more than 32 times, and in every group one expert is named exactly 32 times in the rows of every ep index.
All inputs are finite; a program needn't handle non-finite values.
Results may differ from a plain program's by a relative error of at most 0.0045.
Values may be sent and summed in bfloat16 or wider, within the bound.
A program may use at most 64 MiB of HBM per device.

v0:
```python
import jax
import jax.numpy as jnp
from jax import lax
from jax.sharding import PartitionSpec as P

D = 4096
GROUPS = 4
TOP_K = 2


residual_scale = 2.0**0.5
norm_eps = 1e-05


def on_device(
    tokens, expert_ids, group_weight, expert_weight, w_gate, w_up, w_down, norm_gain, norm_bias
):
    tok_count = tokens.shape[0]
    expert_count = lax.axis_size("ep")
    capacity = min(tok_count // GROUPS, 3 * TOP_K * tok_count // (2 * expert_count))
    pair_count = tok_count * TOP_K
    flat_ids = expert_ids.reshape(pair_count)
    one_hot = (flat_ids[:, None] == jnp.arange(expert_count, dtype=jnp.int32)[None, :]).astype(
        jnp.float32
    )
    earlier = (jnp.arange(pair_count)[:, None] > jnp.arange(pair_count)[None, :]).astype(
        jnp.float32
    )
    prior_counts = jnp.dot(
        earlier, one_hot, preferred_element_type=jnp.float32, precision=lax.Precision.HIGHEST
    )
    slot_index = jnp.sum(prior_counts * one_hot, axis=1).astype(jnp.int32)
    position = flat_ids * capacity + slot_index
    owner_token = jnp.arange(pair_count, dtype=jnp.int32) // TOP_K
    slot_table = (
        jnp.full((expert_count * capacity,), tok_count, jnp.int32).at[position].set(owner_token)
    )
    gate_local = w_gate[0]
    up_local = w_up[0]
    down_local = w_down[0]
    padded = jnp.concatenate([tokens, jnp.zeros((1, tokens.shape[1]), tokens.dtype)], axis=0)
    outgoing = padded[slot_table].reshape(expert_count, capacity, tokens.shape[1])
    arrived = lax.all_to_all(outgoing, "ep", split_axis=0, concat_axis=0, tiled=True)
    sources, slot_count, slice_width = arrived.shape
    row_block = arrived.reshape(sources * slot_count, slice_width)
    row_piece = lax.all_gather(row_block, "tp", axis=1, tiled=True)
    gate_sum = jnp.dot(row_piece, gate_local, preferred_element_type=jnp.float32)
    up_sum = jnp.dot(row_piece, up_local, preferred_element_type=jnp.float32)
    hidden = (jax.nn.silu(gate_sum) * up_sum).astype(jnp.bfloat16)
    result = jnp.dot(
        lax.all_gather(hidden, "tp", axis=1, tiled=True),
        down_local,
        preferred_element_type=jnp.float32,
    )
    result = result.astype(jnp.bfloat16).reshape(sources, slot_count, down_local.shape[1])
    returned = lax.all_to_all(result, "ep", split_axis=0, concat_axis=0, tiled=True)
    flat_rows = returned.reshape(expert_count * capacity, returned.shape[2])
    picked = flat_rows[position].reshape(tok_count, TOP_K, returned.shape[2]).astype(jnp.float32)
    share_weight = (
        group_weight[:, None] * expert_weight / jnp.sum(expert_weight, axis=1, keepdims=True)
    )
    routed = jnp.einsum("tk,tkd->td", share_weight, picked)
    mixed = residual_scale * tokens.astype(jnp.float32) + routed
    first_sum, second_sum = lax.psum((jnp.sum(mixed, axis=1), jnp.sum(mixed * mixed, axis=1)), "tp")
    center = first_sum / D
    spread = second_sum / D - center * center
    centered = mixed - center[:, None]
    normed = (
        centered * lax.rsqrt(spread + norm_eps)[:, None] * norm_gain[None, :] + norm_bias[None, :]
    )
    return normed.astype(jnp.bfloat16)


def solution(mesh):
    return jax.shard_map(
        on_device,
        mesh=mesh,
        in_specs=(
            P("ep", "tp"),
            P("ep", None),
            P("ep"),
            P("ep", None),
            P("ep", None, "tp"),
            P("ep", None, "tp"),
            P("ep", None, "tp"),
            P("tp"),
            P("tp"),
        ),
        out_specs=P("ep", "tp"),
        check_vma=False,
    )
```

profile of v0, /device:TPU:0, one launch (start us, length us, event | category | flops | bytes accessed | tf_op | source)
XLA Modules:
  0.0 102.6 jit_solution(2581811494604423040)
XLA Ops:
  6.5 0.9 copy.11
  7.4 0.7 broadcast_multiply_fusion
  8.1 0.1 eq.15
  8.2 0.2 fusion.1
  8.5 0.1 copy.10
  8.6 0.1 mul.68
  8.7 1.4 %scatter_custom_fusion = s32[256]{0:T(256)S(1)} fusion(s32[256]{0:T(256)S(1)} %bitcast.33, s32[256]{0:T(256)S(1)} %and_select_fusion, s32[]{:T(128)} %constant.31.clone.1), kind=kCustom, calls=%fused_computation.30 | custom fusion | bytes 1028 | tf_op jit(solution)/shard_map/scatter | solution.py:36
  10.1 1.0 concatenate.3
  11.1 1.2 %gather_fusion = bf16[256,1024]{1,0:T(8,128)(2,1)S(1)} fusion(bf16[129,1024]{1,0:T(8,128)(2,1)S(1)} %concatenate.3, s32[1024]{0:T(1024)S(1)} %pad_clamp_fusion.1), kind=kCustom, calls=%fused_computation | custom fusion | bytes 1049600 | tf_op jit(solution)/shard_map/gather | solution.py:42
  12.3 21.7 %all_to_all.10 = bf16[8,32,1024]{2,1,0:T(8,128)(2,1)} all-to-all(bf16[8,32,1024]{2,1,0:T(8,128)(2,1)S(1)} %bitcast.31), channel_id=1, replica_groups=mesh['ep'=8,'tp'=4] {'ep'}, dimensions={0} | all-to-all | bytes 1048576 | tf_op jit(solution)/shard_map/all_to_all | solution.py:43
  34.0 21.8 %all-gather.2.cloned.1.call-done = bf16[256,4096]{1,0:T(8,128)(2,1)} async-done(((bf16[256,1024]{1,0:T(8,128)(2,1)}), bf16[256,4096]{1,0:T(8,128)(2,1)}) %all-gather.2.cloned.1.call-update) | async-done | bytes 2097168 | tf_op jit(solution)/shard_map/all_gather | solution.py:46
  55.8 2.5 %fusion.4 = f32[256,128]{1,0:T(8,128)S(1)} fusion(bf16[256,4096]{1,0:T(8,128)(2,1)} %all-gather.2.cloned.1.call-done, bf16[1,4096,128]{2,1,0:T(8,128)(2,1)S(1)} %copy-done.3), kind=kOutput, calls=%fused_computation.10 | convolution fusion | flops 268435456 | bytes 3276800 | tf_op jit(solution)/shard_map/dot_general | solution.py:47
  58.3 0.7 fusion
  59.0 5.8 %all_gather.7 = bf16[256,512]{1,0:T(8,128)(2,1)S(1)} all-gather(bf16[256,128]{1,0:T(8,128)(2,1)S(1)} %fusion), channel_id=1, replica_groups=mesh['ep'=8,'tp'=4] {'tp'}, dimensions={1}, use_global_device_ids=true | all-gather | bytes 327680 | tf_op jit(solution)/shard_map/all_gather | solution.py:51
  64.8 1.3 %convolution_convert_fusion = bf16[256,1024]{1,0:T(8,128)(2,1)} fusion(bf16[256,512]{1,0:T(8,128)(2,1)S(1)} %all_gather.7, bf16[1,512,1024]{2,1,0:T(8,128)(2,1)S(1)} %copy-done), kind=kOutput, calls=%fused_computation.3 | convolution fusion | flops 268697600 | bytes 1835008 | tf_op jit(solution)/shard_map/dot_general | solution.py:50
  66.1 5.5 %all-to-all-start.1 = ((bf16[8,32,1024]{2,1,0:T(8,128)(2,1)}), bf16[8,32,1024]{2,1,0:T(8,128)(2,1)S(1)}, u32[]{:S(2)}, u32[]{:S(2)}) async-start(bf16[8,32,1024]{2,1,0:T(8,128)(2,1)} %bitcast.8), calls=%async_computation.1 | async-start | bytes 1048576 | tf_op jit(solution)/shard_map/all_to_all | solution.py:56
  71.7 0.1 copy.12
  71.8 14.8 %all-to-all-done.1 = bf16[8,32,1024]{2,1,0:T(8,128)(2,1)S(1)} async-done(((bf16[8,32,1024]{2,1,0:T(8,128)(2,1)}), bf16[8,32,1024]{2,1,0:T(8,128)(2,1)S(1)}, u32[]{:S(2)}, u32[]{:S(2)}) %all-to-all-start.1) | async-done | bytes 524320 | tf_op jit(solution)/shard_map/all_to_all | solution.py:56
  86.6 1.2 %gather_fusion.1 = bf16[256,1024]{1,0:T(8,128)(2,1)S(1)} fusion(bf16[256,1024]{1,0:T(8,128)(2,1)S(1)} %bitcast.30, s32[1024]{0:T(1024)S(1)} %pad_clamp_fusion), kind=kCustom, calls=%fused_computation.1 | custom fusion | bytes 1049600 | tf_op jit(solution)/shard_map/gather | solution.py:58
  87.8 0.2 reshape.59
  88.0 0.7 fusion.10
  88.7 0.2 fusion.6
  88.9 5.9 %all-reduce.1 = (f32[128]{0:T(128)S(1)}, f32[128]{0:T(128)S(1)}) all-reduce(f32[128]{0:T(128)S(1)} %get-tuple-element.6, f32[128]{0:T(128)S(1)} %get-tuple-element.5), channel_id=1, replica_groups=mesh['ep'=8,'tp'=4] {'tp'}, use_global_device_ids=true, to_apply=%region_6.7 | all-reduce | flops 256 | bytes 2048 | tf_op jit(solution)/shard_map/psum | solution.py:64
  94.9 0.9 add_convert_fusion
  (29 shorter events, 0.2 us)
Async XLA Ops:
  6.5 58.3 %copy-start = (bf16[1,512,1024]{2,1,0:T(8,128)(2,1)S(1)}, bf16[1,512,1024]{2,1,0:T(8,128)(2,1)}, u32[]{:S(2)}) copy-start(bf16[1,512,1024]{2,1,0:T(8,128)(2,1)} %param.15) | copy-start | bytes 3145732
  6.5 49.3 %all-gather.2.cloned.1.call-start = ((), (), s32[]{:S(2)}) async-start(), calls=%async_computation.2 | async-start | bytes 2621440 | tf_op jit(solution)/shard_map/all_gather | solution.py:46
  11.1 44.7 %copy-start.3 = (bf16[1,4096,128]{2,1,0:T(8,128)(2,1)S(1)}, bf16[1,4096,128]{2,1,0:T(8,128)(2,1)}, u32[]{:S(2)}) copy-start(bf16[1,4096,128]{2,1,0:T(8,128)(2,1)} %param.13) | copy-start | bytes 3145732
  34.0 24.2 %copy-start.8 = (bf16[1,4096,128]{2,1,0:T(8,128)(2,1)S(1)}, bf16[1,4096,128]{2,1,0:T(8,128)(2,1)}, u32[]{:S(2)}) copy-start(bf16[1,4096,128]{2,1,0:T(8,128)(2,1)} %param.14) | copy-start | bytes 3145732
  55.8 2.5 %copy-start.2 = (bf16[256,4096]{1,0:T(8,128)(2,1)S(1)}, bf16[256,4096]{1,0:T(8,128)(2,1)}, u32[]{:S(2)}) copy-start(bf16[256,4096]{1,0:T(8,128)(2,1)} %all-gather.2.cloned.1.call-done) | copy-start | bytes 6291460
  59.0 12.6 %copy-start.6 = (f32[128,2]{0,1:T(2,128)S(1)}, f32[128,2]{0,1:T(2,128)}, u32[]{:S(2)}) copy-start(f32[128,2]{0,1:T(2,128)} %param.12) | copy-start | bytes 3076
  59.0 12.6 %copy-start.7 = (f32[128]{0:T(128)S(1)}, f32[128]{0:T(128)}, u32[]{:S(2)}) copy-start(f32[128]{0:T(128)} %param.11) | copy-start | bytes 1540
  66.1 20.5 %all-to-all-start.1 = ((bf16[8,32,1024]{2,1,0:T(8,128)(2,1)}), bf16[8,32,1024]{2,1,0:T(8,128)(2,1)S(1)}, u32[]{:S(2)}, u32[]{:S(2)}) async-start(bf16[8,32,1024]{2,1,0:T(8,128)(2,1)} %bitcast.8), calls=%async_computation.1 | async-start | bytes 1048576 | tf_op jit(solution)/shard_map/all_to_all | solution.py:56
  87.8 1.0 copy-start.1
  87.8 7.1 %copy-start.4 = (f32[1024]{0:T(1024)S(1)}, f32[1024]{0:T(1024)}, u32[]{:S(2)}) copy-start(f32[1024]{0:T(1024)} %param.17) | copy-start | bytes 12292
  87.8 7.1 %copy-start.5 = (f32[1024]{0:T(1024)S(1)}, f32[1024]{0:T(1024)}, u32[]{:S(2)}) copy-start(f32[1024]{0:T(1024)} %param.16) | copy-start | bytes 12292
Sparse Core Ops, SparseCore 0:
  34.2 21.5 all-gather.1
where the time goes:
time: 103 us
  waiting for transfers between devices  36.6 us (36%)
  blocking collectives  33.5 us (33%)
  between operations  13.6 us (13%)
  local copies, waits for them, and re-layouts  6.37 us (6%)
  starting transfers between devices  5.51 us (5%)
  matrix products  5.3 us (5%)
  other arithmetic  1.85 us (2%)
    all_gather x1, waiting for transfers between devices, on_device(): row_piece = lax.all_gather(row_block, 'tp', axis=1, tiled=True)  21.8 us
    all_to_all x1, blocking collectives, on_device(): lax.all_to_all(outgoing, 'ep', split_axis=0, concat_axis=0, tiled=True)  21.7 us
    all_to_all x1, waiting for transfers between devices, on_device(): lax.all_to_all(result, 'ep', split_axis=0, concat_axis=0, tiled=True)  14.8 us
    psum x1, blocking collectives, on_device(): lax.psum((jnp.sum(mixed, axis=1), jnp.sum(mixed * mixed, axis=1)), 'tp')  5.93 us
    all_gather x1, blocking collectives, on_device(): lax.all_gather(hidden, 'tp', axis=1, tiled=True)  5.81 us
    all_to_all x1, starting transfers between devices, on_device(): lax.all_to_all(result, 'ep', split_axis=0, concat_axis=0, tiled=True)  5.51 us
    dot_general x1, matrix products, on_device(): jnp.dot(row_piece, gate_local, preferred_element_type=jnp.float32)  2.45 us
  transfers between devices with their start and end apart: 2, of which 2 were waited for; matrix products, arithmetic and copies ran while one was open for 0% of the time, Pallas kernels for 0%

commit v1 on v0

--- a/solution.py
+++ b/solution.py
@@ -1,6 +1,10 @@
+import functools
+
 import jax
 import jax.numpy as jnp
 from jax import lax
+from jax.experimental import pallas as pl
+from jax.experimental.pallas import tpu as pltpu
 from jax.sharding import PartitionSpec as P
 
 D = 4096
@@ -71,9 +75,293 @@
     return normed.astype(jnp.bfloat16)
 
 
+MESH = pl.DeviceIdType.MESH
+F32 = jnp.float32
+BF16 = jnp.bfloat16
+(TO_PLANE, SHARES, CORE_OWN, ACROSS_X, ACROSS_Y, CORE_X, CORE_Y, RELAY_X, RELAY_Y,
+ CORE_RX, CORE_RY, HIDDEN_0, HIDDEN_1, RESULT, BACK, STATS) = range(16)
+KINDS = 16
+
+
+def flip(value, bits):
+    bit = 1
+    while bit <= bits:
+        if bits & bit:
+            value = value + bit - 2 * bit * lax.rem(lax.div(value, bit), 2)
+        bit *= 2
+    return value
+
+
+def layer_kernel(
+    n_plane, n_tp,
+    tokens_ref, ids_ref, group_ref, expert_ref, gate_hbm, up_hbm, down_hbm, gain_ref, bias_ref,
+    out_ref,
+    w_in, w_out, outgoing, share_out, share_in, rows, hidden, own_part, result_out, result_in,
+    back_out, back_in, stats, send_sem, recv_sem, load_sem,
+):
+    ep = lax.axis_index("ep")
+    q = lax.axis_index("tp")
+    z, x = lax.div(ep, 2), lax.rem(ep, 2)
+    ox = 1 - x
+    q_core, q_y, q_diag = flip(q, 1), flip(q, 2), flip(q, 3)
+    core_peer, y_peer, diag_peer = (ep, q_core), (ep, q_y), (ep, q_diag)
+    x_peer = (z * 2 + ox, q)
+
+    def plane_peer(d):
+        return (flip(z, d) * 2 + x, q)
+
+    tok, width = tokens_ref.shape
+    cap = tok // n_plane
+    half = cap // 2
+    inner = gate_hbm.shape[2]
+
+    barrier = pltpu.get_barrier_semaphore()
+    partners = [plane_peer(d) for d in range(1, n_plane)] + [x_peer, core_peer, y_peer, diag_peer]
+    for peer in partners:
+        pl.semaphore_signal(barrier, inc=1, device_id=peer, device_id_type=MESH)
+
+    loads = [
+        pltpu.make_async_copy(gate_hbm.at[0], w_in.at[:, pl.ds(0, inner)], load_sem.at[0]),
+        pltpu.make_async_copy(up_hbm.at[0], w_in.at[:, pl.ds(inner, inner)], load_sem.at[1]),
+        pltpu.make_async_copy(down_hbm.at[0], w_out, load_sem.at[2]),
+    ]
+    for load in loads:
+        load.start()
+
+    first = ids_ref[0:1, :]
+    group_row = (first >> 1).astype(F32)
+    on_lanes = jnp.broadcast_to(group_row, (tok, tok))
+    on_rows = jnp.transpose(on_lanes)
+    ii = lax.broadcasted_iota(jnp.int32, (tok, tok), 0)
+    jj = lax.broadcasted_iota(jnp.int32, (tok, tok), 1)
+    same = on_lanes == on_rows
+    zero, one = jnp.zeros((tok, tok), F32), jnp.ones((tok, tok), F32)
+    rank_row = jnp.sum(jnp.where(same & (ii < jj), one, zero), axis=0, keepdims=True)
+    rank_col = jnp.sum(jnp.where(same & (jj < ii), one, zero), axis=1, keepdims=True)
+    place_row = group_row * cap + rank_row
+    place_col = on_rows[:, 0:1] * cap + rank_col
+    to_slot = jnp.broadcast_to(place_row, (tok, tok)) == ii.astype(F32)
+    to_token = jnp.broadcast_to(place_col, (tok, tok)) == jj.astype(F32)
+
+    sorted_rows = jnp.dot(
+        jnp.where(to_slot, one, zero).astype(BF16), tokens_ref[...], preferred_element_type=F32
+    ).astype(BF16)
+    outgoing[...] = sorted_rows.reshape(n_plane, cap, width)
+    rows[q, x, z] = outgoing[z]
+
+    weights = expert_ref[...]
+    share = group_ref[...] * weights / jnp.sum(weights, axis=0, keepdims=True)
+    even = (first & 1) == 0
+    share_a = jnp.where(even, share[0:1, :], share[1:2, :])
+    share_b = jnp.where(even, share[1:2, :], share[0:1, :])
+    slot_a = jnp.sum(jnp.where(to_slot, jnp.broadcast_to(share_a, (tok, tok)), zero), axis=1, keepdims=True)
+    slot_b = jnp.sum(jnp.where(to_slot, jnp.broadcast_to(share_b, (tok, tok)), zero), axis=1, keepdims=True)
+    lane = lax.broadcasted_iota(jnp.int32, (tok, 128), 1)
+    share_out[...] = jnp.where(lane < 64, slot_a, slot_b).reshape(n_plane, cap, 128)
+    share_in[z] = share_out[z]
+
+    pl.semaphore_wait(barrier, len(partners))
+
+    started = []
+
+    def copy(src, dst, kind, j, peer):
+        return pltpu.make_async_remote_copy(
+            src_ref=src, dst_ref=dst, send_sem=send_sem.at[kind, j], recv_sem=recv_sem.at[kind, j],
+            device_id=peer, device_id_type=MESH,
+        )
+
+    def send(src, dst, kind, j, peer):
+        c = copy(src, dst, kind, j, peer)
+        c.start()
+        started.append(c)
+
+    def arrived(dst, kind, j):
+        copy(dst, dst, kind, j, core_peer).wait_recv()
+
+    for d in range(1, n_plane):
+        send(outgoing.at[flip(z, d)], rows.at[q, x, z], TO_PLANE, d, plane_peer(d))
+
+    low, high = pl.ds(0, half), pl.ds(half, half)
+
+    def spread_own(j):
+        block = rows.at[q, x, flip(z, j)]
+        if j:
+            arrived(block, TO_PLANE, j)
+        send(block, block, ACROSS_X, j, x_peer)
+        send(block, block, ACROSS_Y, j, y_peer)
+        send(block, block, CORE_OWN, j, core_peer)
+
+    def pass_on(j):
+        zz = flip(z, j)
+        block = rows.at[q, ox, zz]
+        arrived(block, ACROSS_X, j)
+        send(block.at[low], block.at[low], RELAY_Y, j, y_peer)
+        send(block, block, CORE_X, j, core_peer)
+        block = rows.at[q_y, x, zz]
+        arrived(block, ACROSS_Y, j)
+        send(block.at[high], block.at[high], RELAY_X, j, x_peer)
+        send(block, block, CORE_Y, j, core_peer)
+
+    def pass_relayed(j):
+        block = rows.at[q_y, ox, flip(z, j)]
+        arrived(block.at[low], RELAY_Y, j)
+        send(block.at[low], block.at[low], CORE_RY, j, core_peer)
+        arrived(block.at[high], RELAY_X, j)
+        send(block.at[high], block.at[high], CORE_RX, j, core_peer)
+
+    for step in range(n_plane + 1):
+        if step < n_plane:
+            spread_own(step)
+        if step == 0:
+            for d in range(1, n_plane):
+                send(share_out.at[flip(z, d)], share_in.at[z], SHARES, d, plane_peer(d))
+        if step >= 1:
+            pass_on(step - 1)
+        if step >= 2:
+            pass_relayed(step - 2)
+
+    def sums_of(column, quarter):
+        part = rows[quarter, column].reshape(tok, width)
+        w = w_in[pl.ds(pl.multiple_of(quarter * width, width), width), :]
+        return jnp.dot(part, w, preferred_element_type=F32)
+
+    def finish_hidden(total, column, kind):
+        gate, up = total[:, :inner], total[:, inner:]
+        hidden[column, q] = (gate / (1.0 + jnp.exp(-gate)) * up).astype(BF16)
+        block = hidden.at[column, q]
+        for d, peer in ((2, y_peer), (3, diag_peer), (1, core_peer)):
+            send(block, block, kind, d, peer)
+
+    def project(column, kind):
+        for d in range(1, n_tp):
+            arrived(hidden.at[column, flip(q, d)], kind, d)
+        h = jnp.concatenate([hidden[column, t] for t in range(n_tp)], axis=1)
+        return jnp.dot(h, w_out[...], preferred_element_type=F32).astype(BF16)
+
+    loads[0].wait()
+    loads[1].wait()
+    total = sums_of(x, q) + sums_of(x, q_y)
+    other = sums_of(ox, q)
+    for j in range(n_plane):
+        arrived(rows.at[q_core, x, flip(z, j)], CORE_OWN, j)
+        arrived(rows.at[q_diag, x, flip(z, j)], CORE_Y, j)
+    total = total + sums_of(x, q_core) + sums_of(x, q_diag)
+    finish_hidden(total, x, HIDDEN_0)
+    pass_relayed(n_plane - 1)
+    for j in range(n_plane):
+        arrived(rows.at[q_core, ox, flip(z, j)], CORE_X, j)
+    other = other + sums_of(ox, q_core) + sums_of(ox, q_y)
+    for j in range(n_plane):
+        block = rows.at[q_diag, ox, flip(z, j)]
+        arrived(block.at[low], CORE_RY, j)
+        arrived(block.at[high], CORE_RX, j)
+    other = other + sums_of(ox, q_diag)
+    finish_hidden(other, ox, HIDDEN_1)
+
+    loads[2].wait()
+    for d in range(1, n_plane):
+        arrived(share_in.at[flip(z, d)], SHARES, d)
+    shares = share_in[...].reshape(tok, 128)
+    is_first = x == 0
+    share_own = jnp.where(is_first, shares[:, 0:1], shares[:, 64:65])
+    share_other = jnp.where(is_first, shares[:, 64:65], shares[:, 0:1])
+    own_part[...] = (project(x, HIDDEN_0).astype(F32) * share_own).reshape(n_plane, cap, width)
+    share_in[...] = jnp.broadcast_to(share_other, (tok, 128)).reshape(n_plane, cap, 128)
+
+    result_out[...] = project(ox, HIDDEN_1).reshape(n_plane, cap, width)
+    order = tuple(range(n_plane - 1, -1, -1))
+    for j in order:
+        zz = flip(z, j)
+        send(result_out.at[zz], result_in.at[zz], RESULT, j, x_peer)
+    for j in order:
+        zz = flip(z, j)
+        arrived(result_in.at[zz], RESULT, j)
+        mixed_rows = own_part[zz] + result_in[zz].astype(F32) * share_in[zz][:, 0:1]
+        if j:
+            back_out[zz] = mixed_rows.astype(BF16)
+            send(back_out.at[zz], back_in.at[z], BACK, j, plane_peer(j))
+        else:
+            back_in[z] = mixed_rows.astype(BF16)
+    for j in order:
+        if j:
+            arrived(back_in.at[flip(z, j)], BACK, j)
+    routed = jnp.dot(
+        jnp.where(to_token, one, zero).astype(BF16),
+        back_in[...].reshape(tok, width),
+        preferred_element_type=F32,
+    )
+    mixed = residual_scale * tokens_ref[...].astype(F32) + routed
+    total_col = jnp.sum(mixed, axis=1, keepdims=True)
+    centered = mixed - total_col / width
+    square_col = jnp.sum(centered * centered, axis=1, keepdims=True)
+    lane = lax.broadcasted_iota(jnp.int32, (tok, 128), 1)
+    stats[q] = jnp.transpose(jnp.where(lane == 0, total_col, square_col))[0:8, :]
+    for d, peer in ((3, diag_peer), (2, y_peer), (1, core_peer)):
+        send(stats.at[q], stats.at[q], STATS, d, peer)
+    for d in range(1, n_tp):
+        arrived(stats.at[flip(q, d)], STATS, d)
+    pieces = [stats[t] for t in range(n_tp)]
+    full = width * n_tp
+    center = sum(p[0:1, :] for p in pieces) / full
+    spread = sum(p[1:2, :] + width * jnp.square(p[0:1, :] / width - center) for p in pieces) / full
+    scale = lax.rsqrt(spread + norm_eps)
+    sub = lax.broadcasted_iota(jnp.int32, (128, tok), 0)
+    columns = jnp.transpose(jnp.where(sub == 0, center, scale))
+    out_ref[...] = (
+        (mixed - columns[:, 0:1]) * columns[:, 1:2] * gain_ref[...] + bias_ref[...]
+    ).astype(BF16)
+    for c in started:
+        c.wait_send()
+
+
+def pair_groups(
+    tokens, expert_ids, group_weight, expert_weight, w_gate, w_up, w_down, norm_gain, norm_bias
+):
+    tok, width = tokens.shape
+    n_plane = lax.axis_size("ep") // TOP_K
+    n_tp = lax.axis_size("tp")
+    cap = tok // n_plane
+    inner = w_gate.shape[2]
+    vmem = pl.BlockSpec(memory_space=pltpu.VMEM)
+    hbm = pl.BlockSpec(memory_space=pltpu.HBM)
+    return pl.pallas_call(
+        functools.partial(layer_kernel, n_plane, n_tp),
+        out_shape=jax.ShapeDtypeStruct((tok, width), BF16),
+        in_specs=[vmem, vmem, vmem, vmem, hbm, hbm, hbm, vmem, vmem],
+        out_specs=vmem,
+        scratch_shapes=[
+            pltpu.VMEM((w_gate.shape[1], 2 * inner), BF16),
+            pltpu.VMEM(w_down.shape[1:], BF16),
+            pltpu.VMEM((n_plane, cap, width), BF16),
+            pltpu.VMEM((n_plane, cap, 128), F32),
+            pltpu.VMEM((n_plane, cap, 128), F32),
+            pltpu.VMEM((n_tp, 2, n_plane, cap, width), BF16),
+            pltpu.VMEM((2, n_tp, tok, inner), BF16),
+            pltpu.VMEM((n_plane, cap, width), F32),
+            pltpu.VMEM((n_plane, cap, width), BF16),
+            pltpu.VMEM((n_plane, cap, width), BF16),
+            pltpu.VMEM((n_plane, cap, width), BF16),
+            pltpu.VMEM((n_plane, cap, width), BF16),
+            pltpu.VMEM((n_tp, 8, tok), F32),
+            pltpu.SemaphoreType.DMA((KINDS, 4)),
+            pltpu.SemaphoreType.DMA((KINDS, 4)),
+            pltpu.SemaphoreType.DMA((3,)),
+        ],
+        compiler_params=pltpu.CompilerParams(
+            collective_id=0, has_side_effects=True, vmem_limit_bytes=56 * 2**20
+        ),
+        name="layer",
+    )(
+        tokens, expert_ids.T, group_weight[None, :], expert_weight.T, w_gate, w_up, w_down,
+        norm_gain[None, :], norm_bias[None, :],
+    )
+
+
 def solution(mesh):
+    n_ep, n_tp = mesh.shape["ep"], mesh.shape["tp"]
+    pairs = TOP_K == 2 and n_ep == GROUPS * TOP_K and n_tp == 4
     return jax.shard_map(
-        on_device,
+        pair_groups if pairs else on_device,
         mesh=mesh,
         in_specs=(
             P("ep", "tp"),

time: 103 us -> 44.2 us (0.43)
  Pallas kernels: 0 us -> 42.3 us
  waiting for transfers between devices: 36.6 us -> 0 us
  blocking collectives: 33.5 us -> 0 us
  between operations: 13.6 us -> 0.01 us
  starting transfers between devices: 5.51 us -> 0 us
  matrix products: 5.3 us -> 0 us
  local copies, waits for them, and re-layouts: 6.37 us -> 1.67 us
  other arithmetic: 1.85 us -> 0 us
    pallas_call x0 -> x1, Pallas kernels: none -> 42.3 us  [pair_groups(): pl.pallas_call(functools.partial(layer_kernel, n_plane, n_tp), out_shape=...]
    all_gather x1 -> x0, waiting for transfers between devices: 21.8 us -> none  [on_device(): row_piece = lax.all_gather(row_block, 'tp', axis=1, tiled=True)]
    all_to_all x1 -> x0, blocking collectives: 21.7 us -> none  [on_device(): lax.all_to_all(outgoing, 'ep', split_axis=0, concat_axis=0, tiled=True)]
    all_to_all x1 -> x0, waiting for transfers between devices: 14.8 us -> none  [on_device(): lax.all_to_all(result, 'ep', split_axis=0, concat_axis=0, tiled=True)]
    psum x1 -> x0, blocking collectives: 5.93 us -> none  [on_device(): lax.psum((jnp.sum(mixed, axis=1), jnp.sum(mixed * mixed, axis=1)), 'tp')]
    all_gather x1 -> x0, blocking collectives: 5.81 us -> none  [on_device(): lax.all_gather(hidden, 'tp', axis=1, tiled=True)]
    all_to_all x1 -> x0, starting transfers between devices: 5.51 us -> none  [on_device(): lax.all_to_all(result, 'ep', split_axis=0, concat_axis=0, tiled=True)]
    dot_general x5 -> x0, matrix products: 5.3 us -> none  [the longest x1 2.45 us: on_device(): jnp.dot(row_piece, gate_local, preferred_element_type=jnp.float32)]
  transfers between devices with their start and end apart: 2 -> 0, of which waited for: 2 -> 0; matrix products, arithmetic and copies ran while one was open for 0% -> 0% of each run, Pallas kernels for 0% -> 0%
where the time goes in v1:
time: 44.2 us; the launch traced here: 44 us
  Pallas kernels  42.3 us (96%)
  local copies, waits for them, and re-layouts  1.67 us (4%)
    pallas_call x1, Pallas kernels, pair_groups(): pl.pallas_call(functools.partial(layer_kernel, n_plane, n_tp), out_shape=...  42.3 us
    unnamed x1, local copies, waits for them, and re-layouts  1.67 us

profile of v1, /device:TPU:0, one launch (start us, length us, event | category | flops | bytes accessed | tf_op | source)
XLA Modules:
  0.0 44.0 jit_solution(10356580396583500882)
XLA Ops:
  0.0 42.3 %layer.1 = bf16[128,1024]{1,0:T(8,128)(2,1)} custom-call(bf16[128,1024]{1,0:T(8,128)(2,1)} %tokens_ref.1, s32[2,128]{1,0:T(2,128)} %bitcast.7, f32[1,128]{1,0:T(1,128)} %bitcast.9, f32[2,128]{1,0:T(2,128)} %bitcast.8, bf16[1,4096,128]{2,1,0:T(8,128)(2,1)} %gate_hbm.1, bf16[1,4096,128]{2,1,0:T(8,128)(2,1)} %up_hbm.1, bf16[1,512,1024]{2,1,0:T(8,128)(2,1)} %down_hbm.1, ...), custom_call_target="tpu_custom_call" | custom-call | tf_op jit(solution)/shard_map/layer/pallas_call | solution.py:327
  42.3 1.7 %copy.11 = bf16[128,1024]{1,0:T(8,128)(2,1)} copy(bf16[128,1024]{1,0:T(8,128)(2,1)} %layer.1) | data formatting | bytes 524288

commit v2 on v1

--- a/solution.py
+++ b/solution.py
@@ -79,8 +79,9 @@
 F32 = jnp.float32
 BF16 = jnp.bfloat16
 (TO_PLANE, SHARES, CORE_OWN, ACROSS_X, ACROSS_Y, CORE_X, CORE_Y, RELAY_X, RELAY_Y,
- CORE_RX, CORE_RY, HIDDEN_0, HIDDEN_1, RESULT, BACK, STATS) = range(16)
-KINDS = 16
+ CORE_RX, CORE_RY, HIDDEN_0, HIDDEN_1, RESULT, BACK, STATS, ACROSS_X2, ACROSS_Y2, RESULT_2,
+ BACK_2) = range(20)
+KINDS = 20
 
 
 def flip(value, bits):
@@ -94,8 +95,9 @@
 
 def layer_kernel(
     n_plane, n_tp,
-    tokens_ref, ids_ref, group_ref, expert_ref, gate_hbm, up_hbm, down_hbm, gain_ref, bias_ref,
-    out_ref,
+    tokens_hbm, ids_hbm, group_hbm, expert_hbm, gate_hbm, up_hbm, down_hbm,
+    mixed_out, columns_out,
+    tokens_ref, ids_ref, group_ref, expert_ref, mixed_ref,
     w_in, w_out, outgoing, share_out, share_in, rows, hidden, own_part, result_out, result_in,
     back_out, back_in, stats, send_sem, recv_sem, load_sem,
 ):
@@ -115,6 +117,16 @@
     half = cap // 2
     inner = gate_hbm.shape[2]
 
+    inputs = [
+        pltpu.make_async_copy(source, target, load_sem.at[3 + i])
+        for i, (source, target) in enumerate((
+            (ids_hbm, ids_ref), (tokens_hbm, tokens_ref), (group_hbm, group_ref),
+            (expert_hbm, expert_ref),
+        ))
+    ]
+    for load in inputs:
+        load.start()
+
     barrier = pltpu.get_barrier_semaphore()
     partners = [plane_peer(d) for d in range(1, n_plane)] + [x_peer, core_peer, y_peer, diag_peer]
     for peer in partners:
@@ -128,6 +140,7 @@
     for load in loads:
         load.start()
 
+    inputs[0].wait()
     first = ids_ref[0:1, :]
     group_row = (first >> 1).astype(F32)
     on_lanes = jnp.broadcast_to(group_row, (tok, tok))
@@ -143,12 +156,15 @@
     to_slot = jnp.broadcast_to(place_row, (tok, tok)) == ii.astype(F32)
     to_token = jnp.broadcast_to(place_col, (tok, tok)) == jj.astype(F32)
 
+    inputs[1].wait()
     sorted_rows = jnp.dot(
         jnp.where(to_slot, one, zero).astype(BF16), tokens_ref[...], preferred_element_type=F32
     ).astype(BF16)
     outgoing[...] = sorted_rows.reshape(n_plane, cap, width)
     rows[q, x, z] = outgoing[z]
 
+    inputs[2].wait()
+    inputs[3].wait()
     weights = expert_ref[...]
     share = group_ref[...] * weights / jnp.sum(weights, axis=0, keepdims=True)
     even = (first & 1) == 0
@@ -187,20 +203,23 @@
         block = rows.at[q, x, flip(z, j)]
         if j:
             arrived(block, TO_PLANE, j)
-        send(block, block, ACROSS_X, j, x_peer)
-        send(block, block, ACROSS_Y, j, y_peer)
+        send(block.at[low], block.at[low], ACROSS_X, j, x_peer)
+        send(block.at[high], block.at[high], ACROSS_Y, j, y_peer)
+        send(block.at[high], block.at[high], ACROSS_X2, j, x_peer)
+        send(block.at[low], block.at[low], ACROSS_Y2, j, y_peer)
         send(block, block, CORE_OWN, j, core_peer)
 
     def pass_on(j):
         zz = flip(z, j)
-        block = rows.at[q, ox, zz]
-        arrived(block, ACROSS_X, j)
-        send(block.at[low], block.at[low], RELAY_Y, j, y_peer)
-        send(block, block, CORE_X, j, core_peer)
-        block = rows.at[q_y, x, zz]
-        arrived(block, ACROSS_Y, j)
-        send(block.at[high], block.at[high], RELAY_X, j, x_peer)
-        send(block, block, CORE_Y, j, core_peer)
+        over_x, over_y = rows.at[q, ox, zz], rows.at[q_y, x, zz]
+        arrived(over_x.at[low], ACROSS_X, j)
+        send(over_x.at[low], over_x.at[low], RELAY_Y, j, y_peer)
+        arrived(over_y.at[high], ACROSS_Y, j)
+        send(over_y.at[high], over_y.at[high], RELAY_X, j, x_peer)
+        arrived(over_x.at[high], ACROSS_X2, j)
+        send(over_x, over_x, CORE_X, j, core_peer)
+        arrived(over_y.at[low], ACROSS_Y2, j)
+        send(over_y, over_y, CORE_Y, j, core_peer)
 
     def pass_relayed(j):
         block = rows.at[q_y, ox, flip(z, j)]
@@ -212,13 +231,13 @@
     for step in range(n_plane + 1):
         if step < n_plane:
             spread_own(step)
-        if step == 0:
-            for d in range(1, n_plane):
-                send(share_out.at[flip(z, d)], share_in.at[z], SHARES, d, plane_peer(d))
         if step >= 1:
             pass_on(step - 1)
         if step >= 2:
             pass_relayed(step - 2)
+
+    for d in range(1, n_plane):
+        send(share_out.at[flip(z, d)], share_in.at[z], SHARES, d, plane_peer(d))
 
     def sums_of(column, quarter):
         part = rows[quarter, column].reshape(tok, width)
@@ -270,27 +289,35 @@
 
     result_out[...] = project(ox, HIDDEN_1).reshape(n_plane, cap, width)
     order = tuple(range(n_plane - 1, -1, -1))
+    pieces = ((low, 0, RESULT, BACK), (high, half, RESULT_2, BACK_2))
     for j in order:
         zz = flip(z, j)
-        send(result_out.at[zz], result_in.at[zz], RESULT, j, x_peer)
+        for part, _, there, _ in pieces:
+            send(result_out.at[zz, part], result_in.at[zz, part], there, j, x_peer)
     for j in order:
         zz = flip(z, j)
-        arrived(result_in.at[zz], RESULT, j)
-        mixed_rows = own_part[zz] + result_in[zz].astype(F32) * share_in[zz][:, 0:1]
-        if j:
-            back_out[zz] = mixed_rows.astype(BF16)
-            send(back_out.at[zz], back_in.at[z], BACK, j, plane_peer(j))
-        else:
-            back_in[z] = mixed_rows.astype(BF16)
+        for part, at, there, home in pieces:
+            arrived(result_in.at[zz, part], there, j)
+            scaled = result_in[zz, at:at + half].astype(F32) * share_in[zz, at:at + half][:, 0:1]
+            mixed_rows = (own_part[zz, at:at + half] + scaled).astype(BF16)
+            if j:
+                back_out[zz, at:at + half] = mixed_rows
+                send(back_out.at[zz, part], back_in.at[z, part], home, j, plane_peer(j))
+            else:
+                back_in[z, at:at + half] = mixed_rows
     for j in order:
         if j:
-            arrived(back_in.at[flip(z, j)], BACK, j)
+            for part, _, _, home in pieces:
+                arrived(back_in.at[flip(z, j), part], home, j)
     routed = jnp.dot(
         jnp.where(to_token, one, zero).astype(BF16),
         back_in[...].reshape(tok, width),
         preferred_element_type=F32,
     )
     mixed = residual_scale * tokens_ref[...].astype(F32) + routed
+    mixed_ref[...] = mixed
+    keep = pltpu.make_async_copy(mixed_ref, mixed_out, load_sem.at[7])
+    keep.start()
     total_col = jnp.sum(mixed, axis=1, keepdims=True)
     centered = mixed - total_col / width
     square_col = jnp.sum(centered * centered, axis=1, keepdims=True)
@@ -306,12 +333,17 @@
     spread = sum(p[1:2, :] + width * jnp.square(p[0:1, :] / width - center) for p in pieces) / full
     scale = lax.rsqrt(spread + norm_eps)
     sub = lax.broadcasted_iota(jnp.int32, (128, tok), 0)
-    columns = jnp.transpose(jnp.where(sub == 0, center, scale))
-    out_ref[...] = (
-        (mixed - columns[:, 0:1]) * columns[:, 1:2] * gain_ref[...] + bias_ref[...]
-    ).astype(BF16)
+    columns_out[...] = jnp.transpose(jnp.where(sub == 0, center, scale))
+    keep.wait()
     for c in started:
         c.wait_send()
+
+
+def norm_kernel(mixed_ref, columns_ref, gain_ref, bias_ref, out_ref):
+    center, scale = columns_ref[:, 0:1], columns_ref[:, 1:2]
+    out_ref[...] = (
+        (mixed_ref[...] - center) * scale * gain_ref[...] + bias_ref[...]
+    ).astype(BF16)
 
 
 def pair_groups(
@@ -324,12 +356,19 @@
     inner = w_gate.shape[2]
     vmem = pl.BlockSpec(memory_space=pltpu.VMEM)
     hbm = pl.BlockSpec(memory_space=pltpu.HBM)
-    return pl.pallas_call(
+    mixed, columns = pl.pallas_call(
         functools.partial(layer_kernel, n_plane, n_tp),
-        out_shape=jax.ShapeDtypeStruct((tok, width), BF16),
-        in_specs=[vmem, vmem, vmem, vmem, hbm, hbm, hbm, vmem, vmem],
-        out_specs=vmem,
+        out_shape=(
+            jax.ShapeDtypeStruct((tok, width), F32), jax.ShapeDtypeStruct((tok, 128), F32)
+        ),
+        in_specs=[hbm] * 7,
+        out_specs=(pl.BlockSpec(memory_space=pl.ANY), vmem),
         scratch_shapes=[
+            pltpu.VMEM((tok, width), BF16),
+            pltpu.VMEM((TOP_K, tok), jnp.int32),
+            pltpu.VMEM((1, tok), F32),
+            pltpu.VMEM((TOP_K, tok), F32),
+            pltpu.VMEM((tok, width), F32),
             pltpu.VMEM((w_gate.shape[1], 2 * inner), BF16),
             pltpu.VMEM(w_down.shape[1:], BF16),
             pltpu.VMEM((n_plane, cap, width), BF16),
@@ -345,16 +384,23 @@
             pltpu.VMEM((n_tp, 8, tok), F32),
             pltpu.SemaphoreType.DMA((KINDS, 4)),
             pltpu.SemaphoreType.DMA((KINDS, 4)),
-            pltpu.SemaphoreType.DMA((3,)),
+            pltpu.SemaphoreType.DMA((8,)),
         ],
         compiler_params=pltpu.CompilerParams(
             collective_id=0, has_side_effects=True, vmem_limit_bytes=56 * 2**20
         ),
         name="layer",
     )(
-        tokens, expert_ids.T, group_weight[None, :], expert_weight.T, w_gate, w_up, w_down,
-        norm_gain[None, :], norm_bias[None, :],
-    )
+        tokens, expert_ids.T, group_weight[None, :], expert_weight.T, w_gate, w_up, w_down
+    )
+    return pl.pallas_call(
+        norm_kernel,
+        out_shape=jax.ShapeDtypeStruct((tok, width), BF16),
+        in_specs=[vmem] * 4,
+        out_specs=vmem,
+        compiler_params=pltpu.CompilerParams(vmem_limit_bytes=56 * 2**20),
+        name="norm",
+    )(mixed, columns, norm_gain[None, :], norm_bias[None, :])
 
 
 def solution(mesh):

time: 44.2 us -> 42.7 us (0.966)
  local copies, waits for them, and re-layouts: 1.67 us -> 0 us
    pallas_call x0 -> x1, Pallas kernels: none -> 1.95 us  [pair_groups(): pl.pallas_call(norm_kernel, out_shape=jax.ShapeDtypeStruct((tok, width),...]
    pallas_call x1, Pallas kernels: 42.3 us -> 40.6 us  [pair_groups(): pl.pallas_call(functools.partial(layer_kernel, n_plane, n_tp), out_shape=...]
    unnamed x1 -> x0, local copies, waits for them, and re-layouts: 1.67 us -> none
where the time goes in v2:
time: 42.7 us; the launch traced here: 42.5 us
  Pallas kernels  42.5 us (100%)
    pallas_call x1, Pallas kernels, pair_groups(): pl.pallas_call(functools.partial(layer_kernel, n_plane, n_tp), out_shape=...  40.6 us
    pallas_call x1, Pallas kernels, pair_groups(): pl.pallas_call(norm_kernel, out_shape=jax.ShapeDtypeStruct((tok, width),...  1.95 us

profile of v2, /device:TPU:0, one launch (start us, length us, event | category | flops | bytes accessed | tf_op | source)
XLA Modules:
  0.0 42.5 jit_solution(9484045076748368330)
XLA Ops:
  0.0 40.6 %layer.1 = (f32[128,1024]{1,0:T(8,128)}, f32[128,128]{1,0:T(8,128)}) custom-call(bf16[128,1024]{1,0:T(8,128)(2,1)} %tokens_hbm.1, s32[2,128]{1,0:T(2,128)} %bitcast.7, f32[1,128]{1,0:T(1,128)} %bitcast.9, f32[2,128]{1,0:T(2,128)} %bitcast.8, bf16[1,4096,128]{2,1,0:T(8,128)(2,1)} %gate_hbm.1, bf16[1,4096,128]{2,1,0:T(8,128)(2,1)} %up_hbm.1, ...), custom_call_target="tpu_custom_call" | custom-call | tf_op jit(solution)/shard_map/layer/pallas_call | solution.py:359
  40.6 2.0 %norm.1 = bf16[128,1024]{1,0:T(8,128)(2,1)} custom-call(f32[128,1024]{1,0:T(8,128)} %get-tuple-element.7.mixed_ref, f32[128,128]{1,0:T(8,128)} %get-tuple-element.8.columns_ref, f32[1,1024]{1,0:T(1,128)} %bitcast.5, f32[1,1024]{1,0:T(1,128)} %bitcast.6), custom_call_target="tpu_custom_call" | custom-call | tf_op jit(solution)/shard_map/norm/pallas_call | solution.py:396

commit v3 on v2

--- a/solution.py
+++ b/solution.py
@@ -80,8 +80,8 @@
 BF16 = jnp.bfloat16
 (TO_PLANE, SHARES, CORE_OWN, ACROSS_X, ACROSS_Y, CORE_X, CORE_Y, RELAY_X, RELAY_Y,
  CORE_RX, CORE_RY, HIDDEN_0, HIDDEN_1, RESULT, BACK, STATS, ACROSS_X2, ACROSS_Y2, RESULT_2,
- BACK_2) = range(20)
-KINDS = 20
+ BACK_2, TO_PLANE_2) = range(21)
+KINDS = 21
 
 
 def flip(value, bits):
@@ -194,19 +194,23 @@
     def arrived(dst, kind, j):
         copy(dst, dst, kind, j, core_peer).wait_recv()
 
+    low, high = pl.ds(0, half), pl.ds(half, half)
     for d in range(1, n_plane):
-        send(outgoing.at[flip(z, d)], rows.at[q, x, z], TO_PLANE, d, plane_peer(d))
-
-    low, high = pl.ds(0, half), pl.ds(half, half)
+        for part, kind in ((low, TO_PLANE), (high, TO_PLANE_2)):
+            send(outgoing.at[flip(z, d), part], rows.at[q, x, z, part], kind, d, plane_peer(d))
 
     def spread_own(j):
         block = rows.at[q, x, flip(z, j)]
         if j:
-            arrived(block, TO_PLANE, j)
+            arrived(block.at[low], TO_PLANE, j)
         send(block.at[low], block.at[low], ACROSS_X, j, x_peer)
+        if j:
+            send(block.at[low], block.at[low], ACROSS_Y2, j, y_peer)
+            arrived(block.at[high], TO_PLANE_2, j)
         send(block.at[high], block.at[high], ACROSS_Y, j, y_peer)
         send(block.at[high], block.at[high], ACROSS_X2, j, x_peer)
-        send(block.at[low], block.at[low], ACROSS_Y2, j, y_peer)
+        if not j:
+            send(block.at[low], block.at[low], ACROSS_Y2, j, y_peer)
         send(block, block, CORE_OWN, j, core_peer)
 
     def pass_on(j):
@@ -387,7 +391,7 @@
             pltpu.SemaphoreType.DMA((8,)),
         ],
         compiler_params=pltpu.CompilerParams(
-            collective_id=0, has_side_effects=True, vmem_limit_bytes=56 * 2**20
+            collective_id=0, has_side_effects=True, vmem_limit_bytes=53 * 2**20
         ),
         name="layer",
     )(
@@ -398,7 +402,7 @@
         out_shape=jax.ShapeDtypeStruct((tok, width), BF16),
         in_specs=[vmem] * 4,
         out_specs=vmem,
-        compiler_params=pltpu.CompilerParams(vmem_limit_bytes=56 * 2**20),
+        compiler_params=pltpu.CompilerParams(vmem_limit_bytes=8 * 2**20),
         name="norm",
     )(mixed, columns, norm_gain[None, :], norm_bias[None, :])
 

time: 42.7 us -> 42.7 us (level)
  local copies, waits for them, and re-layouts: 0 us -> 1.65 us
  Pallas kernels: 42.5 us -> 40.9 us
    unnamed x0 -> x12, local copies, waits for them, and re-layouts: none -> 1.65 us
    pallas_call x1, Pallas kernels: 1.95 us -> 0.87 us  [pair_groups(): pl.pallas_call(norm_kernel, out_shape=jax.ShapeDtypeStruct((tok, width),...]
    pallas_call x1, Pallas kernels: 40.6 us -> 40 us  [pair_groups(): pl.pallas_call(functools.partial(layer_kernel, n_plane, n_tp), out_shape=...]
where the time goes in v3:
time: 42.7 us; the launch traced here: 42.6 us
  Pallas kernels  40.9 us (96%)
  local copies, waits for them, and re-layouts  1.65 us (4%)
    pallas_call x1, Pallas kernels, pair_groups(): pl.pallas_call(functools.partial(layer_kernel, n_plane, n_tp), out_shape=...  40 us
    unnamed x12, local copies, waits for them, and re-layouts  1.65 us
    pallas_call x1, Pallas kernels, pair_groups(): pl.pallas_call(norm_kernel, out_shape=jax.ShapeDtypeStruct((tok, width),...  0.87 us

profile of v3, /device:TPU:0, one launch (start us, length us, event | category | flops | bytes accessed | tf_op | source)
XLA Modules:
  0.0 42.6 jit_solution(17253677646286027632)
XLA Ops:
  0.0 0.0 copy-start.4
  0.0 0.0 copy-start.3
  0.0 0.0 copy-start.5
  0.0 0.7 %copy-done.4 = f32[128,2]{0,1:T(2,128)S(1)} copy-done((f32[128,2]{0,1:T(2,128)S(1)}, f32[128,2]{0,1:T(2,128)}, u32[]{:S(2)}) %copy-start.4) | copy-done | bytes 1048
  0.7 0.0 copy-done.3
  0.7 0.0 copy-done.5
  0.7 0.0 copy-start
  0.7 0.9 %copy-done = bf16[128,1024]{1,0:T(8,128)(2,1)S(1)} copy-done((bf16[128,1024]{1,0:T(8,128)(2,1)S(1)}, bf16[128,1024]{1,0:T(8,128)(2,1)}, u32[]{:S(2)}) %copy-start) | copy-done | bytes 262168
  1.6 0.0 copy-start.1
  1.7 0.0 copy-start.2
  1.7 40.0 %layer.1 = (f32[128,1024]{1,0:T(8,128)S(1)}, f32[128,128]{1,0:T(8,128)S(1)}) custom-call(bf16[128,1024]{1,0:T(8,128)(2,1)S(1)} %copy-done, s32[2,128]{1,0:T(2,128)S(1)} %bitcast.7, f32[1,128]{1,0:T(1,128)S(1)} %bitcast.9, f32[2,128]{1,0:T(2,128)S(1)} %bitcast.8, bf16[1,4096,128]{2,1,0:T(8,128)(2,1)} %gate_hbm.1, bf16[1,4096,128]{2,1,0:T(8,128)(2,1)} %up_hbm.1, ...), custom_call_target="tpu_custom_call" | custom-call | tf_op jit(solution)/shard_map/layer/pallas_call | solution.py:363
  41.7 0.0 copy-done.1
  41.7 0.0 copy-done.2
  41.7 0.9 %norm.1 = bf16[128,1024]{1,0:T(8,128)(2,1)} custom-call(f32[128,1024]{1,0:T(8,128)S(1)} %get-tuple-element.7.mixed_ref, f32[128,128]{1,0:T(8,128)S(1)} %get-tuple-element.8.columns_ref, f32[1,1024]{1,0:T(1,128)S(1)} %bitcast.5, f32[1,1024]{1,0:T(1,128)S(1)} %bitcast.6), custom_call_target="tpu_custom_call" | custom-call | tf_op jit(solution)/shard_map/norm/pallas_call | solution.py:400
Async XLA Ops:
  0.0 0.7 %copy-start.4 = (f32[128,2]{0,1:T(2,128)S(1)}, f32[128,2]{0,1:T(2,128)}, u32[]{:S(2)}) copy-start(f32[128,2]{0,1:T(2,128)} %param.12) | copy-start | bytes 3076
  0.0 0.7 %copy-start.3 = (s32[128,2]{0,1:T(2,128)S(1)}, s32[128,2]{0,1:T(2,128)}, u32[]{:S(2)}) copy-start(s32[128,2]{0,1:T(2,128)} %param.10) | copy-start | bytes 3076
  0.0 0.7 %copy-start.5 = (f32[128]{0:T(128)S(1)}, f32[128]{0:T(128)}, u32[]{:S(2)}) copy-start(f32[128]{0:T(128)} %param.11) | copy-start | bytes 1540
  0.7 1.0 %copy-start = (bf16[128,1024]{1,0:T(8,128)(2,1)S(1)}, bf16[128,1024]{1,0:T(8,128)(2,1)}, u32[]{:S(2)}) copy-start(bf16[128,1024]{1,0:T(8,128)(2,1)} %tokens_hbm.1) | copy-start | bytes 786436
  1.6 40.0 %copy-start.1 = (f32[1024]{0:T(1024)S(1)}, f32[1024]{0:T(1024)}, u32[]{:S(2)}) copy-start(f32[1024]{0:T(1024)} %param.16) | copy-start | bytes 12292
  1.7 40.0 %copy-start.2 = (f32[1024]{0:T(1024)S(1)}, f32[1024]{0:T(1024)}, u32[]{:S(2)}) copy-start(f32[1024]{0:T(1024)} %param.17) | copy-start | bytes 12292

commit v4 on v3

--- a/solution.py
+++ b/solution.py
@@ -395,7 +395,12 @@
         ),
         name="layer",
     )(
-        tokens, expert_ids.T, group_weight[None, :], expert_weight.T, w_gate, w_up, w_down
+        *(
+            pltpu.with_memory_space_constraint(a, pltpu.HBM)
+            for a in (
+                tokens, expert_ids.T, group_weight[None, :], expert_weight.T, w_gate, w_up, w_down
+            )
+        )
     )
     return pl.pallas_call(
         norm_kernel,

time: 42.7 us -> 41.2 us (0.965)
  local copies, waits for them, and re-layouts: 1.65 us -> 0.01 us
    unnamed x12 -> x4, local copies, waits for them, and re-layouts: 1.65 us -> 0.01 us
where the time goes in v4:
time: 41.2 us; the launch traced here: 41.1 us
  Pallas kernels  41.1 us (100%)
    pallas_call x1, Pallas kernels, pair_groups(): pl.pallas_call(functools.partial(layer_kernel, n_plane, n_tp), out_shape=...  40.2 us
    pallas_call x1, Pallas kernels, pair_groups(): pl.pallas_call(norm_kernel, out_shape=jax.ShapeDtypeStruct((tok, width),...  0.87 us

profile of v4, /device:TPU:0, one launch (start us, length us, event | category | flops | bytes accessed | tf_op | source)
XLA Modules:
  0.0 41.1 jit_solution(4371462433319868708)
XLA Ops:
  0.0 0.0 copy-start
  0.0 0.0 copy-start.1
  0.0 40.2 %layer.1 = (f32[128,1024]{1,0:T(8,128)S(1)}, f32[128,128]{1,0:T(8,128)S(1)}) custom-call(bf16[128,1024]{1,0:T(8,128)(2,1)} %tokens_hbm.1, s32[2,128]{1,0:T(2,128)} %bitcast.7, f32[1,128]{1,0:T(1,128)} %bitcast.9, f32[2,128]{1,0:T(2,128)} %bitcast.8, bf16[1,4096,128]{2,1,0:T(8,128)(2,1)} %gate_hbm.1, bf16[1,4096,128]{2,1,0:T(8,128)(2,1)} %up_hbm.1, ...), custom_call_target="tpu_custom_call" | custom-call | tf_op jit(solution)/shard_map/layer/pallas_call | solution.py:363
  40.2 0.0 copy-done
  40.2 0.0 copy-done.1
  40.2 0.9 %norm.1 = bf16[128,1024]{1,0:T(8,128)(2,1)} custom-call(f32[128,1024]{1,0:T(8,128)S(1)} %get-tuple-element.7.mixed_ref, f32[128,128]{1,0:T(8,128)S(1)} %get-tuple-element.8.columns_ref, f32[1,1024]{1,0:T(1,128)S(1)} %bitcast.5, f32[1,1024]{1,0:T(1,128)S(1)} %bitcast.6), custom_call_target="tpu_custom_call" | custom-call | tf_op jit(solution)/shard_map/norm/pallas_call | solution.py:405
Async XLA Ops:
  0.0 40.2 %copy-start = (f32[1024]{0:T(1024)S(1)}, f32[1024]{0:T(1024)}, u32[]{:S(2)}) copy-start(f32[1024]{0:T(1024)} %param.16) | copy-start | bytes 12292
  0.0 40.2 %copy-start.1 = (f32[1024]{0:T(1024)S(1)}, f32[1024]{0:T(1024)}, u32[]{:S(2)}) copy-start(f32[1024]{0:T(1024)} %param.17) | copy-start | bytes 12292
